TPU v7x, 32 devices: a whole 2x2x4 slice. The times are simulated.
32 devices in a mesh: grp: 2 (over y), kv: 4 (over z), tp: 4 (over x, core).
Axes of the slice: x: 2, y: 2, z: 4, core: 2. Of those that a mesh axis runs over, the one named last changes fastest.
Arguments:
- tokens: bfloat16 [16, 4096], P('grp', 'kv'), parts along dimension 0, may hold values from -6 to 6
- norm_gain: float32 [4096], replicated, may hold values from 0.1 to 1.9
- w_query: bfloat16 [4096, 4096], P('kv', 'tp'), may hold values from -0.09375 to 0.09375
- key_weight: bfloat16 [4096, 512], P('kv', 'tp'), may hold values from -0.09375 to 0.09375
- value_weight: bfloat16 [4096, 512], P('kv', 'tp'), may hold values from -0.09375 to 0.09375
- w_gate: bfloat16 [4096, 64], replicated, may hold values from -0.09375 to 0.09375
- gate_bias: float32 [64], replicated, may hold values from -3 to 4
- w_out: bfloat16 [4096, 4096], P('kv', 'tp'), may hold values from -0.1875 to 0.1875
- cache_keys: bfloat16 [16, 3072, 512], P('grp', 'kv', 'tp'), parts along dimension 0, may hold values from -240 to 240
- cache_values: bfloat16 [16, 3072, 512], P('grp', 'kv', 'tp'), parts along dimension 0, may hold values from -8 to 8
- cache_gate: float32 [16, 64, 3072], P('grp', 'tp', 'kv'), parts along dimension 0, may hold values from -3072 to 0, as said below
- gate_total: float32 [16, 64], P('grp', 'tp'), parts along dimension 0, may hold values from -3072 to 0, as said below
- lengths: int32 [16], P('grp'), parts along dimension 0, may hold values from 1536 to 3072, as said below
Outputs:
- mixed: bfloat16 [16, 4096], P('grp', 'kv'), parts along dimension 0
- key_new: bfloat16 [16, 512], P('grp', 'tp'), parts along dimension 0
- value_new: bfloat16 [16, 512], P('grp', 'tp'), parts along dimension 0
There are 2 independent parts, one for each index of `grp`. A program takes and returns all parts, laid end to end along the dimension named above; an argument that names none is the same for every part. Nothing has to cross between parts.
Inputs may be any that keep to these rules, and one draw needn't show every extreme that they name: `lengths`: one sequence of each draw has all 3072 positions cached. `cache_gate`: non-increasing along positions. `gate_total`: equal to cache_gate at position lengths - 1 of the same sequence and head.
All inputs are finite; a program needn't handle non-finite values.
Results may differ from a plain program's by a relative error of at most 0.015.
Values may be sent and summed in bfloat16 or wider, within the bound.
A program may use at most 64 MiB of HBM per device.

v0:
```python
import jax
import jax.numpy as jnp
from jax import lax
from jax.sharding import PartitionSpec as P

HEAD_SIZE = 64


NEG_FILL = -1e30


def per_device(
    tokens,
    norm_gain,
    w_query,
    key_weight,
    value_weight,
    w_gate,
    gate_bias,
    w_out,
    cache_keys,
    cache_values,
    cache_gate,
    gate_total,
    lengths,
):
    seq_count = tokens.shape[0]
    width_dev = tokens.shape[1]
    heads_dev = cache_gate.shape[1]
    positions_dev = cache_gate.shape[2]
    kv_heads_dev = cache_keys.shape[2] // HEAD_SIZE
    head_group = heads_dev // kv_heads_dev
    logit_scale = HEAD_SIZE ** (-0.5)
    whole = lax.all_gather(tokens, "kv", axis=1, tiled=True)
    features = whole.astype(jnp.float32)
    normed = (
        features
        * lax.rsqrt(jnp.mean(features * features, axis=-1, keepdims=True) + 1e-06)
        * norm_gain
    )
    normed = normed.astype(jnp.bfloat16)
    kv_index = lax.axis_index("kv")
    tp_index = lax.axis_index("tp")
    own_rows = lax.dynamic_slice_in_dim(normed, kv_index * width_dev, width_dev, 1)
    query_part = jnp.dot(own_rows, w_query, preferred_element_type=jnp.float32)
    key_part = jnp.dot(own_rows, key_weight, preferred_element_type=jnp.float32)
    value_part = jnp.dot(own_rows, value_weight, preferred_element_type=jnp.float32)
    query_sum, key_sum, value_sum = lax.psum((query_part, key_part, value_part), "kv")
    query = query_sum.astype(jnp.bfloat16)
    key_new = key_sum.astype(jnp.bfloat16)
    value_new = value_sum.astype(jnp.bfloat16)
    gate_cols = lax.dynamic_slice_in_dim(w_gate, tp_index * heads_dev, heads_dev, 1)
    bias_cols = lax.dynamic_slice_in_dim(gate_bias, tp_index * heads_dev, heads_dev, 0)
    log_gate = jax.nn.log_sigmoid(
        jnp.dot(normed, gate_cols, preferred_element_type=jnp.float32) + bias_cols
    )
    level = gate_total + log_gate
    query_head_rows = query.reshape(seq_count, kv_heads_dev, head_group, HEAD_SIZE)
    key_block = cache_keys.reshape(seq_count, positions_dev, kv_heads_dev, HEAD_SIZE)
    value_block = cache_values.reshape(seq_count, positions_dev, kv_heads_dev, HEAD_SIZE)
    score_matrix = (
        jnp.einsum(
            "skgd,spkd->skgp", query_head_rows, key_block, preferred_element_type=jnp.float32
        )
        * logit_scale
    )
    forget_bias = (level[:, :, None] - cache_gate).reshape(
        seq_count, kv_heads_dev, head_group, positions_dev
    )
    positions = kv_index * positions_dev + jnp.arange(positions_dev, dtype=jnp.int32)
    valid_mask = (positions[None, :] < lengths[:, None])[:, None, None, :]
    score_matrix = jnp.where(valid_mask, score_matrix + forget_bias, NEG_FILL)
    local_max = jnp.max(score_matrix, axis=-1)
    weights = jnp.where(valid_mask, jnp.exp(score_matrix - local_max[..., None]), 0.0)
    local_total = jnp.sum(weights, axis=-1)
    local_values = jnp.einsum(
        "skgp,spkd->skgd",
        weights.astype(jnp.bfloat16),
        value_block,
        preferred_element_type=jnp.float32,
    )
    block_max = lax.pmax(local_max, "kv")
    rescale = jnp.exp(local_max - block_max)
    block_total, block_values = lax.psum(
        (local_total * rescale, local_values * rescale[..., None]), "kv"
    )
    key_current = key_new.reshape(seq_count, kv_heads_dev, HEAD_SIZE)
    current_score = (
        jnp.einsum(
            "skgd,skd->skg", query_head_rows, key_current, preferred_element_type=jnp.float32
        )
        * logit_scale
    )
    top = jnp.maximum(block_max, current_score)
    cached_scale = jnp.exp(block_max - top)
    current_weight = jnp.exp(current_score - top)
    denominator = block_total * cached_scale + current_weight
    value_current = value_new.reshape(seq_count, kv_heads_dev, 1, HEAD_SIZE).astype(jnp.float32)
    total_sum = block_values * cached_scale[..., None] + current_weight[..., None] * value_current
    attended = (
        (total_sum / denominator[..., None])
        .reshape(seq_count, heads_dev * HEAD_SIZE)
        .astype(jnp.bfloat16)
    )
    partial_value = lax.dot_general(
        attended, w_out, (((1,), (1,)), ((), ())), preferred_element_type=jnp.float32
    )
    partial_value = lax.optimization_barrier(partial_value.astype(jnp.bfloat16)).astype(jnp.float32)
    mixed = lax.psum(partial_value.astype(jnp.bfloat16), "tp")
    return (mixed, key_new, value_new)


def solution(mesh):
    placed = (
        P("grp", "kv"),
        P(),
        P("kv", "tp"),
        P("kv", "tp"),
        P("kv", "tp"),
        P(),
        P(),
        P("kv", "tp"),
        P("grp", "kv", "tp"),
        P("grp", "kv", "tp"),
        P("grp", "tp", "kv"),
        P("grp", "tp"),
        P("grp"),
    )
    return jax.shard_map(
        per_device,
        mesh=mesh,
        in_specs=placed,
        out_specs=(P("grp", "kv"), P("grp", "tp"), P("grp", "tp")),
        check_vma=False,
    )
```

profile of v0, /device:TPU:0, one launch (start us, length us, event | category | flops | bytes accessed | tf_op | source)
XLA Modules:
  0.0 91.3 jit_solution(11908319094124294041)
XLA Ops:
  0.6 0.0 copy-start
  0.7 0.9 dynamic_slice.11
  1.5 0.7 broadcast_compare_fusion
  2.3 15.1 %all_gather.3 = bf16[8,4096]{1,0:T(8,128)(2,1)S(1)} all-gather(bf16[8,1024]{1,0:T(8,128)(2,1)} %param.13), channel_id=1, replica_groups=mesh['grp'=2,'kv'=4,'tp'=4] {'kv'}, dimensions={1}, use_global_device_ids=true | all-gather | bytes 81920 | tf_op jit(solution)/shard_map/all_gather | solution.py:34
  17.4 0.1 fusion.9
  17.5 0.8 fusion.11
  18.4 1.1 %fusion.22 = f32[8,16]{1,0:T(8,128)S(1)} fusion(f32[8,16]{1,0:T(8,128)} %param.24, bf16[8,4096]{1,0:T(8,128)(2,1)S(1)} %fusion.11, bf16[4096,64]{0,1:T(8,128)(2,1)} %param.18, s32[]{:T(128)S(6)} %select_n.20, f32[16]{0:T(128)S(1)} %dynamic_slice.11), kind=kOutput, calls=%fused_computation.35 | convolution fusion | flops 1049856 | bytes 201284 | tf_op jit(solution)/shard_map/dot_general | solution.py:55
  19.4 1.1 %fusion.15 = f32[8,128]{1,0:T(8,128)S(1)} fusion(bf16[1024,128]{1,0:T(8,128)(2,1)} %param.16, bf16[8,4096]{1,0:T(8,128)(2,1)S(1)} %fusion.11, s32[]{:T(128)S(6)} %select_n.19), kind=kOutput, calls=%fused_computation.24 | convolution fusion | flops 2097152 | bytes 282628 | tf_op jit(solution)/shard_map/dot_general | solution.py:46
  20.6 1.1 %fusion.13 = f32[8,128]{1,0:T(8,128)S(1)} fusion(bf16[1024,128]{1,0:T(8,128)(2,1)} %param.17, bf16[8,4096]{1,0:T(8,128)(2,1)S(1)} %fusion.11, s32[]{:T(128)S(6)} %select_n.19), kind=kOutput, calls=%fused_computation.22 | convolution fusion | flops 2097152 | bytes 282628 | tf_op jit(solution)/shard_map/dot_general | solution.py:47
  21.7 0.0 copy-done
  21.7 0.4 fusion.17
  22.0 19.1 %psum.42 = bf16[8,1024]{1,0:T(8,128)(2,1)S(1)} all-reduce(f32[8,1024]{1,0:T(8,128)S(1)} %fusion.17), channel_id=1, replica_groups=mesh['grp'=2,'kv'=4,'tp'=4] {'kv'}, use_global_device_ids=true, to_apply=%region_1.0 | all-reduce | flops 8192 | bytes 49152 | tf_op jit(solution)/shard_map/psum | solution.py:48
  41.2 0.1 reshape.76
  41.3 0.0 copy-start.1
  41.3 2.7 %copy.18 = bf16[8,768,128]{1,2,0:T(8,128)(2,1)} copy(bf16[8,768,128]{2,1,0:T(8,128)(2,1)} %param.21) | data formatting | bytes 3145728 | tf_op args[8]
  43.9 0.0 copy-done.1
  43.9 1.8 %fusion.33 = (f32[8,2,8]{2,1,0:T(2,128)S(1)}, f32[8,2,8,768]{3,2,1,0:T(8,128)S(1)}) fusion(f32[8,16,768]{2,1,0:T(8,128)S(1)} %copy-done.1, f32[8,16]{1,0:T(8,128)S(1)} %fusion.22, bf16[8,2,8,64]{3,2,1,0:T(8,128)(2,1)S(1)} %reshape.76, bf16[8,768,2,64]{1,3,2,0:T(8,128)(2,1)} %bitcast.24, pred[8,768]{1,0:T(8,128)(4,1)S(1)} %broadcast_compare_fusion), kind=kOutput, calls=%fused_computation.44 | convolution fusion | flops 13074304 | bytes 2382848 | tf_op jit(solution)/shard_map/skgd,spkd->skgp/dot_general | solution.py:62
  45.7 8.5 %pmax.7 = f32[8,2,8]{2,1,0:T(2,128)S(1)} all-reduce(f32[8,2,8]{2,1,0:T(2,128)S(1)} %get-tuple-element.12), channel_id=1, replica_groups=mesh['grp'=2,'kv'=4,'tp'=4] {'kv'}, use_global_device_ids=true, to_apply=%region_3.0 | all-reduce | flops 128 | bytes 1024 | tf_op jit(solution)/shard_map/pmax | solution.py:82
  54.3 0.2 fusion.3
  54.5 2.6 %copy.19 = bf16[8,768,128]{1,2,0:T(8,128)(2,1)} copy(bf16[8,768,128]{2,1,0:T(8,128)(2,1)} %param.22) | data formatting | bytes 3145728 | tf_op args[9]
  57.1 2.0 %convolution_multiply_fusion.1 = f32[8,2,8,64]{3,2,1,0:T(8,128)S(1)} fusion(bf16[8,768,2,64]{1,3,2,0:T(8,128)(2,1)} %bitcast.25, f32[8,2,8,768]{3,2,1,0:T(8,128)S(1)} %get-tuple-element.13, f32[8,2,8]{2,1,0:T(2,128)S(1)} %get-tuple-element.12, pred[8,768]{1,0:T(8,128)(4,1)S(1)} %broadcast_compare_fusion, f32[8,2,8]{2,1,0:T(2,128)S(1)} %bitcast.30), kind=kOutput, calls=%fused_computation.3 | convolution fusion | flops 12886016 | bytes 2006016 | tf_op jit(solution)/shard_map/skgp,spkd->skgd/dot_general | solution.py:76
  59.1 18.7 %all-reduce = (f32[8,2,8,64]{3,2,1,0:T(8,128)S(1)}, bf16[8,128]{1,0:T(8,128)(2,1)S(1)}, f32[8,2,8]{2,1,0:T(2,128)S(1)}, bf16[8,128]{1,0:T(8,128)(2,1)S(1)}) all-reduce(f32[8,2,8,64]{3,2,1,0:T(8,128)S(1)} %convolution_multiply_fusion.1, f32[8,128]{1,0:T(8,128)S(1)} %fusion.15, ...), channel_id=1, replica_groups=mesh['grp'=2,'kv'=4,'tp'=4] {'kv'}, use_global_device_ids=true, to_apply=%region_4.5 | all-reduce | flops 10368 | bytes 78848 | tf_op jit(solution)/shard_map/psum | solution.py:84
  77.8 0.0 copy-start.2
  77.8 0.0 copy-start.3
  77.8 0.1 reshape.85
  77.9 0.1 fusion.34
  78.1 0.1 reshape.81
  78.1 0.1 divide_convert_fusion
  78.3 0.1 convert_element_type.49
  78.4 2.2 %convolution_convert_fusion = bf16[8,1024]{1,0:T(8,128)(2,1)S(1)} fusion(bf16[8,1024]{1,0:T(8,128)(2,1)S(1)} %convert_element_type.49, bf16[1024,1024]{1,0:T(8,128)(2,1)} %param.20), kind=kOutput, calls=%fused_computation.4 | convolution fusion | flops 16785408 | bytes 2129920 | tf_op jit(solution)/shard_map/dot_general | solution.py:105
  80.6 10.7 %psum.47 = bf16[8,1024]{1,0:T(8,128)(2,1)} all-reduce(bf16[8,1024]{1,0:T(8,128)(2,1)S(1)} %convolution_convert_fusion), channel_id=1, replica_groups=mesh['grp'=2,'kv'=4,'tp'=4] {'tp'}, use_global_device_ids=true, to_apply=%region_9.10 | all-reduce | flops 8192 | bytes 32768 | tf_op jit(solution)/shard_map/psum | solution.py:109
  91.3 0.0 copy-done.2
  91.3 0.0 copy-done.3
  (4 shorter events, 0.1 us)
Async XLA Ops:
  0.6 21.0 %copy-start = (bf16[1024,1024]{1,0:T(8,128)(2,1)S(1)}, bf16[1024,1024]{1,0:T(8,128)(2,1)}, u32[]{:S(2)}) copy-start(bf16[1024,1024]{1,0:T(8,128)(2,1)} %param.15) | copy-start | bytes 6291460
  41.3 2.7 %copy-start.1 = (f32[8,16,768]{2,1,0:T(8,128)S(1)}, f32[8,16,768]{2,1,0:T(8,128)}, u32[]{:S(2)}) copy-start(f32[8,16,768]{2,1,0:T(8,128)} %param.23) | copy-start | bytes 1179652
  77.8 13.5 %copy-start.2 = (bf16[8,128]{1,0:T(8,128)(2,1)}, bf16[8,128]{1,0:T(8,128)(2,1)S(1)}, u32[]{:S(2)}) copy-start(bf16[8,128]{1,0:T(8,128)(2,1)S(1)} %get-tuple-element.4) | copy-start | bytes 6148
  77.8 13.5 %copy-start.3 = (bf16[8,128]{1,0:T(8,128)(2,1)}, bf16[8,128]{1,0:T(8,128)(2,1)S(1)}, u32[]{:S(2)}) copy-start(bf16[8,128]{1,0:T(8,128)(2,1)S(1)} %get-tuple-element.6) | copy-start | bytes 6148
where the time goes:
time: 91.8 us; the launch traced here: 91.3 us
  blocking collectives  72.2 us (79%)
  matrix products  9.82 us (11%)
  local copies, waits for them, and re-layouts  6.53 us (7%)
  other arithmetic  2.09 us (2%)
    psum x1, blocking collectives, per_device(): lax.psum((query_part, key_part, value_part), 'kv')  19.1 us
    psum x1, blocking collectives, per_device(): lax.psum((local_total * rescale, local_values * rescale[..., None]), 'kv')  18.7 us
    all_gather x1, blocking collectives, per_device(): whole = lax.all_gather(tokens, 'kv', axis=1, tiled=True)  15.1 us
    psum x1, blocking collectives, per_device(): mixed = lax.psum(partial_value.astype(jnp.bfloat16), 'tp')  10.7 us
    pmax x1, blocking collectives, per_device(): block_max = lax.pmax(local_max, 'kv')  8.5 us
    unnamed x10, local copies, waits for them, and re-layouts  5.29 us
    dot_general x1, matrix products, per_device(): lax.dot_general(attended, w_out, (((1,), (1,)), ((), ())), preferred_elem...  2.23 us
    dot_general x1, matrix products, per_device(): jnp.einsum('skgp,spkd->skgd', weights.astype(jnp.bfloat16), value_block,...  1.98 us

commit v1 on v0

v1 whole, which is shorter than its diff:
```python
import functools

import jax
import jax.numpy as jnp
from jax import lax
from jax.experimental import pallas as pl
from jax.experimental.pallas import tpu as pltpu
from jax.sharding import PartitionSpec as P

HEAD_SIZE = 64
NEG_FILL = -1e30
LANES = 128
SUBLANES = 8
UNROLL_PEERS = 8
QUERY_PIECES = 4
CACHE_PIECES = 4
NT = (((1,), (1,)), ((), ()))


def fold(count, body, carry):
    if count <= UNROLL_PEERS:
        for i in range(count):
            carry = body(i, carry)
        return carry
    return lax.fori_loop(0, count, body, carry)


def kernel(
    n_kv,
    n_tp,
    tokens_hbm,
    gain_hbm,
    query_hbm,
    key_hbm,
    value_hbm,
    gate_hbm,
    bias_hbm,
    out_hbm,
    keys_hbm,
    values_hbm,
    cgate_hbm,
    total_hbm,
    lengths_hbm,
    mixed_ref,
    knew_ref,
    vnew_ref,
    tokens_v,
    gain_v,
    query_v,
    key_v,
    value_v,
    gate_v,
    bias_v,
    out_v,
    keys_v,
    values_v,
    cgate_v,
    total_v,
    lengths_s,
    parts,
    blocks,
    stats,
    mixes,
    qrows,
    arows,
    square,
    loc,
    send1,
    recv1,
    send2,
    recv2,
    send3,
    recv3,
    send4,
    recv4,
):
    seqs, width = tokens_v.shape
    _, heads, positions = cgate_v.shape
    group = heads // 2
    qcols = query_v.shape[1]
    kcols = key_v.shape[1]
    all_heads = gate_v.shape[1]
    kv = lax.axis_index("kv")
    tp = lax.axis_index("tp")

    barrier = pltpu.get_barrier_semaphore()

    def greet(axis, me, n):
        def one(k, c):
            pl.semaphore_signal(
                barrier,
                inc=1,
                device_id={axis: lax.rem(me + 1 + k, n)},
                device_id_type=pl.DeviceIdType.MESH,
            )
            return c

        fold(n - 1, one, 0)

    greet("kv", kv, n_kv)
    greet("tp", tp, n_tp)

    slot = [0]

    def load(src, dst):
        copy = pltpu.make_async_copy(src, dst, loc.at[slot[0]])
        slot[0] += 1
        copy.start()
        return copy

    c_tokens = load(tokens_hbm, tokens_v)
    c_gain = load(gain_hbm, gain_v)
    rows = pl.ds(pl.multiple_of(kv * width, width), width)
    c_gate = load(gate_hbm.at[rows], gate_v)
    step = width // QUERY_PIECES
    c_query = [
        load(query_hbm.at[pl.ds(i * step, step)], query_v.at[pl.ds(i * step, step)])
        for i in range(QUERY_PIECES)
    ]
    c_key = load(key_hbm, key_v)
    c_value = load(value_hbm, value_v)
    c_bias = load(bias_hbm, bias_v)
    c_total = load(total_hbm, total_v)
    c_lengths = load(lengths_hbm, lengths_s)
    c_cgate = load(cgate_hbm, cgate_v)
    per = seqs // CACHE_PIECES
    c_keys = [
        load(keys_hbm.at[pl.ds(i * per, per)], keys_v.at[pl.ds(i * per, per)])
        for i in range(CACHE_PIECES)
    ]
    c_values = [
        load(values_hbm.at[pl.ds(i * per, per)], values_v.at[pl.ds(i * per, per)])
        for i in range(CACHE_PIECES)
    ]
    c_out = load(out_hbm, out_v)

    def exchange(axis, me, n, buf, send, recv):
        def one(k, c):
            pltpu.make_async_remote_copy(
                src_ref=buf.at[me],
                dst_ref=buf.at[me],
                send_sem=send.at[k],
                recv_sem=recv.at[me],
                device_id={axis: lax.rem(me + 1 + k, n)},
                device_id_type=pl.DeviceIdType.MESH,
            ).start()
            return c

        fold(n - 1, one, 0)

    def arrive(axis, me, n, buf, send, recv):
        def one(k, c):
            peer = lax.rem(me + 1 + k, n)
            copy = pltpu.make_async_remote_copy(
                src_ref=buf.at[me],
                dst_ref=buf.at[peer],
                send_sem=send.at[k],
                recv_sem=recv.at[peer],
                device_id={axis: peer},
                device_id_type=pl.DeviceIdType.MESH,
            )
            copy.wait()
            return c

        fold(n - 1, one, 0)

    lane = lax.broadcasted_iota(jnp.int32, (SUBLANES, LANES), 1)
    low = lane < HEAD_SIZE
    place = lane % HEAD_SIZE

    c_tokens.wait()
    c_gain.wait()
    x = tokens_v[...].astype(jnp.float32)
    squares = jnp.sum(x * x, axis=1, keepdims=True)
    if gain_v.shape[0] == 1:
        scaled = x * gain_v[...]
    else:
        chunks = width // LANES
        scaled = jnp.concatenate(
            [
                x[:, i * LANES : (i + 1) * LANES] * gain_v[pl.ds(kv * chunks + i, 1), :]
                for i in range(chunks)
            ],
            axis=1,
        )
    high = scaled.astype(jnp.bfloat16)
    rest = (scaled - high.astype(jnp.float32)).astype(jnp.bfloat16)
    both = jnp.concatenate([high, rest], axis=0)

    def project(weights, lhs=both):
        out = jnp.dot(lhs, weights, preferred_element_type=jnp.float32)
        return out[:seqs] + out[seqs:]

    c_gate.wait()
    gates = project(gate_v[...])
    base = qcols + 2 * kcols
    pair = jnp.concatenate(
        [gates, jnp.broadcast_to(squares, (seqs, LANES - all_heads))], axis=1
    )
    pair_high = pair.astype(jnp.bfloat16)
    parts[kv, :, base : base + LANES] = pair_high
    parts[kv, :, base + LANES : base + 2 * LANES] = (
        pair - pair_high.astype(jnp.float32)
    ).astype(jnp.bfloat16)
    acc = None
    for i in range(QUERY_PIECES):
        c_query[i].wait()
        cut = slice(i * step, (i + 1) * step)
        term = jnp.dot(both[:, cut], query_v[cut, :], preferred_element_type=jnp.float32)
        acc = term if acc is None else acc + term
    parts[kv, :, :qcols] = (acc[:seqs] + acc[seqs:]).astype(jnp.bfloat16)
    c_key.wait()
    parts[kv, :, qcols : qcols + kcols] = project(key_v[...]).astype(jnp.bfloat16)
    c_value.wait()
    parts[kv, :, qcols + kcols : base] = project(value_v[...]).astype(jnp.bfloat16)

    pl.semaphore_wait(barrier, n_kv - 1 + n_tp - 1)
    exchange("kv", kv, n_kv, parts, send1, recv1)

    c_total.wait()
    c_lengths.wait()
    c_cgate.wait()
    c_bias.wait()
    square[...] = jnp.zeros_like(square)
    square[:seqs, :heads] = total_v[...]
    total_t = jnp.transpose(square[...])[:heads, :]
    index = kv * positions + lax.broadcasted_iota(jnp.int32, (heads, positions), 1)
    for s in range(seqs):
        cgate_v[s] = jnp.where(
            index < lengths_s[s], total_t[:, s : s + 1] - cgate_v[s], NEG_FILL
        )

    arrive("kv", kv, n_kv, parts, send1, recv1)
    summed = fold(
        n_kv,
        lambda j, c: c + parts[j].astype(jnp.float32),
        jnp.zeros((seqs, base + 2 * LANES), jnp.float32),
    )
    pair = summed[:, base : base + LANES] + summed[:, base + LANES :]
    scale = lax.rsqrt(pair[:, all_heads : all_heads + 1] / (width * n_kv) + 1e-6)
    query = (summed[:, :qcols] * scale).astype(jnp.bfloat16).astype(jnp.float32)
    query = query * (HEAD_SIZE ** -0.5)
    knew = (summed[:, qcols : qcols + kcols] * scale).astype(jnp.bfloat16)
    vnew = (summed[:, qcols + kcols : base] * scale).astype(jnp.bfloat16)
    knew_ref[...] = knew
    vnew_ref[...] = vnew
    knew = knew.astype(jnp.float32)
    vnew = vnew.astype(jnp.float32)

    half = heads // 2
    for c in range(half):
        chunk = query[:, c * LANES : (c + 1) * LANES]
        turned = pltpu.roll(chunk, HEAD_SIZE, 1)
        if 2 * c < group:
            even, odd = jnp.where(low, chunk, 0.0), jnp.where(low, turned, 0.0)
        else:
            even, odd = jnp.where(low, 0.0, turned), jnp.where(low, 0.0, chunk)
        qrows[pl.ds(2 * c * seqs, seqs), :] = even
        qrows[pl.ds((2 * c + 1) * seqs, seqs), :] = odd

    def select(column):
        return jnp.where(low, column[:group], column[group:])

    stat = jnp.zeros((group, LANES), jnp.float32)
    held = None
    for s in range(seqs):
        if s % per == 0:
            c_keys[s // per].wait()
        q = qrows[pl.ds(s, heads, stride=seqs), :].astype(jnp.bfloat16)
        score = lax.dot_general(q, keys_v[s], NT, preferred_element_type=jnp.float32)
        score = score + cgate_v[s]
        peak = jnp.max(score, axis=1, keepdims=True)
        weight = jnp.exp(score - peak)
        mass = jnp.sum(weight, axis=1, keepdims=True)
        if s % per == 0:
            c_values[s // per].wait()
        value = jnp.dot(
            weight.astype(jnp.bfloat16), values_v[s], preferred_element_type=jnp.float32
        )
        stat = jnp.where(place == s, select(peak), stat)
        stat = jnp.where(place == seqs + s, select(mass), stat)
        mine = select(value)
        if s % 2 == 0:
            held = mine
        else:
            blocks[kv, (s - 1) * group : (s + 1) * group, :] = jnp.concatenate(
                [held, mine], axis=0
            ).astype(jnp.bfloat16)
    stats[kv] = stat
    exchange("kv", kv, n_kv, stats, send3, recv3)
    exchange("kv", kv, n_kv, blocks, send2, recv2)

    z = pair * scale
    z = z[:, :all_heads] + bias_v[...]
    z = jnp.minimum(z, 0.0) - jnp.log1p(jnp.exp(-jnp.abs(z)))
    square[:seqs, :all_heads] = z
    turned = pltpu.roll(square[:seqs, :], lax.rem(LANES - tp * heads, LANES), 1)
    square[:seqs, :] = turned
    z_t = jnp.transpose(square[...])
    log_gate = jnp.where(low, z_t[:group], pltpu.roll(z_t[group:heads], HEAD_SIZE, 1))
    own = jnp.zeros((group, LANES), jnp.float32)
    for s in range(seqs):
        q = qrows[pl.ds(s, heads, stride=seqs), :]
        own = jnp.where(
            place == s,
            select(jnp.sum(q * knew[s : s + 1, :], axis=1, keepdims=True)),
            own,
        )

    arrive("kv", kv, n_kv, stats, send3, recv3)
    peak = fold(
        n_kv - 1, lambda j, c: jnp.maximum(c, stats[j + 1]), stats[0]
    )
    top = jnp.maximum(peak + log_gate, own)
    own_weight = jnp.exp(own - top)

    def factor(j):
        return jnp.exp(stats[j] + (log_gate - top))

    shift = LANES - seqs
    denominator = fold(
        n_kv, lambda j, c: c + factor(j) * pltpu.roll(stats[j], shift, 1), own_weight
    )
    inverse = 1.0 / denominator

    def spread(a, s):
        return jnp.where(low, a[:, s : s + 1], a[:, HEAD_SIZE + s : HEAD_SIZE + s + 1])

    own_weight = own_weight * inverse
    sums = [spread(own_weight, s) * vnew[s : s + 1, :] for s in range(seqs)]
    arrive("kv", kv, n_kv, blocks, send2, recv2)

    def add(j, sums):
        a = factor(j) * inverse
        block = blocks[j].astype(jnp.float32)
        return [
            sums[s] + spread(a, s) * block[s * group : (s + 1) * group]
            for s in range(seqs)
        ]

    sums = fold(n_kv, add, sums)
    for s in range(seqs):
        arows[pl.ds(s * group, group), :] = sums[s]
    pieces = []
    for c in range(half):
        g = 2 * c % group
        first = arows[pl.ds(g, seqs, stride=group), :]
        second = arows[pl.ds(g + 1, seqs, stride=group), :]
        if 2 * c < group:
            pieces.append(jnp.where(low, first, pltpu.roll(second, HEAD_SIZE, 1)))
        else:
            pieces.append(jnp.where(low, pltpu.roll(first, HEAD_SIZE, 1), second))
    attended = jnp.concatenate(pieces, axis=1).astype(jnp.bfloat16)

    c_out.wait()
    mixes[tp] = lax.dot_general(
        attended, out_v[...], NT, preferred_element_type=jnp.float32
    ).astype(jnp.bfloat16)
    exchange("tp", tp, n_tp, mixes, send4, recv4)
    arrive("tp", tp, n_tp, mixes, send4, recv4)
    total = fold(
        n_tp,
        lambda j, c: c + mixes[j].astype(jnp.float32),
        jnp.zeros((seqs, width), jnp.float32),
    )
    mixed_ref[...] = total.astype(jnp.bfloat16)


def per_device(n_kv, n_tp, *args):
    (
        tokens,
        norm_gain,
        w_query,
        key_weight,
        value_weight,
        w_gate,
        gate_bias,
        w_out,
        cache_keys,
        cache_values,
        cache_gate,
        gate_total,
        lengths,
    ) = args
    seqs, width = tokens.shape
    _, heads, positions = cache_gate.shape
    qcols, kcols = w_query.shape[1], key_weight.shape[1]
    all_heads = w_gate.shape[1]
    if width % LANES == 0:
        gain = norm_gain.reshape(-1, LANES)
    else:
        start = lax.axis_index("kv") * width
        gain = lax.dynamic_slice_in_dim(norm_gain, start, width, 0).reshape(1, width)
    bias = gate_bias.reshape(1, all_heads)
    operands = (
        tokens,
        gain,
        w_query,
        key_weight,
        value_weight,
        w_gate,
        bias,
        w_out,
        cache_keys,
        cache_values,
        cache_gate,
        gate_total,
        lengths,
    )
    bf16, f32 = jnp.bfloat16, jnp.float32
    packed = qcols + 2 * kcols + 2 * LANES
    group = heads // 2
    n_loads = 10 + QUERY_PIECES + 2 * CACHE_PIECES
    dma = pltpu.SemaphoreType.DMA
    return pl.pallas_call(
        functools.partial(kernel, n_kv, n_tp),
        out_shape=(
            jax.ShapeDtypeStruct((seqs, width), bf16),
            jax.ShapeDtypeStruct((seqs, kcols), bf16),
            jax.ShapeDtypeStruct((seqs, kcols), bf16),
        ),
        in_specs=[pl.BlockSpec(memory_space=pl.ANY)] * len(operands),
        out_specs=(pl.BlockSpec(memory_space=pltpu.VMEM),) * 3,
        scratch_shapes=[
            pltpu.VMEM(tokens.shape, bf16),
            pltpu.VMEM(gain.shape, f32),
            pltpu.VMEM(w_query.shape, bf16),
            pltpu.VMEM(key_weight.shape, bf16),
            pltpu.VMEM(value_weight.shape, bf16),
            pltpu.VMEM((width, all_heads), bf16),
            pltpu.VMEM(bias.shape, f32),
            pltpu.VMEM(w_out.shape, bf16),
            pltpu.VMEM(cache_keys.shape, bf16),
            pltpu.VMEM(cache_values.shape, bf16),
            pltpu.VMEM(cache_gate.shape, f32),
            pltpu.VMEM(gate_total.shape, f32),
            pltpu.SMEM(lengths.shape, jnp.int32),
            pltpu.VMEM((n_kv, seqs, packed), bf16),
            pltpu.VMEM((n_kv, seqs * group, LANES), bf16),
            pltpu.VMEM((n_kv, group, LANES), f32),
            pltpu.VMEM((n_tp, seqs, width), bf16),
            pltpu.VMEM((heads * seqs, LANES), f32),
            pltpu.VMEM((seqs * group, LANES), f32),
            pltpu.VMEM((LANES, LANES), f32),
            dma((n_loads,)),
            dma((n_kv,)),
            dma((n_kv,)),
            dma((n_kv,)),
            dma((n_kv,)),
            dma((n_kv,)),
            dma((n_kv,)),
            dma((n_tp,)),
            dma((n_tp,)),
        ],
        compiler_params=pltpu.CompilerParams(
            collective_id=0, has_side_effects=True, vmem_limit_bytes=48 * 1024 * 1024
        ),
    )(*operands)


def solution(mesh):
    placed = (
        P("grp", "kv"),
        P(),
        P("kv", "tp"),
        P("kv", "tp"),
        P("kv", "tp"),
        P(),
        P(),
        P("kv", "tp"),
        P("grp", "kv", "tp"),
        P("grp", "kv", "tp"),
        P("grp", "tp", "kv"),
        P("grp", "tp"),
        P("grp"),
    )
    return jax.shard_map(
        functools.partial(per_device, mesh.shape["kv"], mesh.shape["tp"]),
        mesh=mesh,
        in_specs=placed,
        out_specs=(P("grp", "kv"), P("grp", "tp"), P("grp", "tp")),
        check_vma=False,
    )
```

time: 91.8 us -> 33.3 us (0.36)
  blocking collectives: 72.2 us -> 0 us
  Pallas kernels: 0 us -> 21.1 us
  matrix products: 9.82 us -> 0 us
  local copies, waits for them, and re-layouts: 6.53 us -> 11.1 us
  other arithmetic: 2.09 us -> 0 us
    psum x3 -> x0, blocking collectives: 48.5 us -> none  [the longest x1 19.1 us: per_device(): lax.psum((query_part, key_part, value_part), 'kv')]
    pallas_call x0 -> x1, Pallas kernels: none -> 21.1 us  [per_device(): pl.pallas_call(functools.partial(kernel, n_kv, n_tp), out_shape=(jax.Shap...]
    all_gather x1 -> x0, blocking collectives: 15.1 us -> none  [per_device(): whole = lax.all_gather(tokens, 'kv', axis=1, tiled=True)]
    dot_general x8 -> x0, matrix products: 9.82 us -> none  [the longest x1 2.23 us: per_device(): lax.dot_general(attended, w_out, (((1,), (1,)), ((), ())), preferred_elem...]
    pmax x1 -> x0, blocking collectives: 8.5 us -> none  [per_device(): block_max = lax.pmax(local_max, 'kv')]
    unnamed x10 -> x24, local copies, waits for them, and re-layouts: 5.29 us -> 11.1 us
    convert_element_type x2 -> x0, other arithmetic: 0.92 us -> none  [the longest x1 0.81 us: per_device(): normed = normed.astype(jnp.bfloat16)]
where the time goes in v1:
time: 33.3 us; the launch traced here: 32.9 us
  Pallas kernels  21.1 us (63%)
  local copies, waits for them, and re-layouts  11.1 us (33%)
  between operations  0.68 us (2%)
    pallas_call x1, Pallas kernels, per_device(): pl.pallas_call(functools.partial(kernel, n_kv, n_tp), out_shape=(jax.Shap...  21.1 us
    unnamed x24, local copies, waits for them, and re-layouts  11.1 us

profile of v1, /device:TPU:0, one launch (start us, length us, event | category | flops | bytes accessed | tf_op | source)
XLA Modules:
  0.0 32.9 jit_solution(18178140613747193675)
XLA Ops:
  0.6 0.0 copy-start
  0.6 1.6 %copy.16.gate_hbm = bf16[4096,64]{1,0:T(8,128)(2,1)S(1)} copy(bf16[4096,64]{0,1:T(8,128)(2,1)} %param.18) | data formatting | bytes 1048576 | tf_op args[5]
  2.3 0.0 copy-done
  2.3 0.0 copy-start.1
  2.3 1.4 %copy-done.1 = bf16[8,768,128]{2,1,0:T(8,128)(2,1)S(1)} copy-done((bf16[8,768,128]{2,1,0:T(8,128)(2,1)S(1)}, bf16[8,768,128]{2,1,0:T(8,128)(2,1)}, u32[]{:S(2)}) %copy-start.1) | copy-done | bytes 1572888
  3.7 0.0 copy-start.2
  3.7 1.0 %copy-done.2 = f32[8,16,768]{2,1,0:T(8,128)S(1)} copy-done((f32[8,16,768]{2,1,0:T(8,128)S(1)}, f32[8,16,768]{2,1,0:T(8,128)}, u32[]{:S(2)}) %copy-start.2) | copy-done | bytes 393240
  4.7 0.0 copy-start.3
  4.7 0.9 %copy-done.3 = bf16[1024,128]{1,0:T(8,128)(2,1)S(1)} copy-done((bf16[1024,128]{1,0:T(8,128)(2,1)S(1)}, bf16[1024,128]{1,0:T(8,128)(2,1)}, u32[]{:S(2)}) %copy-start.3) | copy-done | bytes 262168
  5.6 0.0 copy-start.4
  5.7 0.9 %copy-done.4 = bf16[1024,128]{1,0:T(8,128)(2,1)S(1)} copy-done((bf16[1024,128]{1,0:T(8,128)(2,1)S(1)}, bf16[1024,128]{1,0:T(8,128)(2,1)}, u32[]{:S(2)}) %copy-start.4) | copy-done | bytes 262168
  6.6 0.0 copy-start.5
  6.6 0.7 %copy-done.5 = bf16[8,1024]{1,0:T(8,128)(2,1)S(1)} copy-done((bf16[8,1024]{1,0:T(8,128)(2,1)S(1)}, bf16[8,1024]{1,0:T(8,128)(2,1)}, u32[]{:S(2)}) %copy-start.5) | copy-done | bytes 16408
  7.3 0.0 copy-start.6
  7.3 0.7 %copy-done.6 = f32[4096]{0:T(1024)S(1)} copy-done((f32[4096]{0:T(1024)S(1)}, f32[4096]{0:T(1024)}, u32[]{:S(2)}) %copy-start.6) | copy-done | bytes 16408
  8.0 0.0 copy-start.7
  8.0 0.7 %copy-done.7 = f32[8,16]{1,0:T(8,128)S(1)} copy-done((f32[8,16]{1,0:T(8,128)S(1)}, f32[8,16]{1,0:T(8,128)}, u32[]{:S(2)}) %copy-start.7) | copy-done | bytes 536
  8.7 0.0 copy-start.8
  8.7 0.7 %copy-done.8 = f32[64]{0:T(128)S(1)} copy-done((f32[64]{0:T(128)S(1)}, f32[64]{0:T(128)}, u32[]{:S(2)}) %copy-start.8) | copy-done | bytes 280
  9.4 0.0 copy-start.9
  9.4 0.7 %copy-done.9 = s32[8]{0:T(128)S(1)} copy-done((s32[8]{0:T(128)S(1)}, s32[8]{0:T(128)}, u32[]{:S(2)}) %copy-start.9) | copy-done | bytes 56
  10.0 21.1 %shard_map.148 = (bf16[8,1024]{1,0:T(8,128)(2,1)S(1)}, bf16[8,128]{1,0:T(8,128)(2,1)S(1)}, bf16[8,128]{1,0:T(8,128)(2,1)S(1)}) custom-call(bf16[8,1024]{1,0:T(8,128)(2,1)S(1)} %copy-done.5, f32[32,128]{1,0:T(8,128)S(1)} %bitcast.2, bf16[1024,1024]{1,0:T(8,128)(2,1)} %query_hbm.1, bf16[1024,128]{1,0:T(8,128)(2,1)S(1)} %copy-done.3, ...), custom_call_target="tpu_custom_call" | custom-call | tf_op jit(solution)/shard_map/pallas_call | solution.py:415
  31.1 0.6 %copy.20 = bf16[8,1024]{1,0:T(8,128)(2,1)} copy(bf16[8,1024]{1,0:T(8,128)(2,1)S(1)} %get-tuple-element.6) | data formatting | bytes 32768
  31.8 0.6 %copy.21 = bf16[8,128]{1,0:T(8,128)(2,1)} copy(bf16[8,128]{1,0:T(8,128)(2,1)S(1)} %get-tuple-element.7) | data formatting | bytes 4096
  32.3 0.6 %copy.22 = bf16[8,128]{1,0:T(8,128)(2,1)} copy(bf16[8,128]{1,0:T(8,128)(2,1)S(1)} %get-tuple-element.8) | data formatting | bytes 4096
Async XLA Ops:
  0.6 1.7 %copy-start = (bf16[8,768,128]{2,1,0:T(8,128)(2,1)S(1)}, bf16[8,768,128]{2,1,0:T(8,128)(2,1)}, u32[]{:S(2)}) copy-start(bf16[8,768,128]{2,1,0:T(8,128)(2,1)} %keys_hbm.1) | copy-start | bytes 4718596
  2.3 1.4 %copy-start.1 = (bf16[8,768,128]{2,1,0:T(8,128)(2,1)S(1)}, bf16[8,768,128]{2,1,0:T(8,128)(2,1)}, u32[]{:S(2)}) copy-start(bf16[8,768,128]{2,1,0:T(8,128)(2,1)} %values_hbm.1) | copy-start | bytes 4718596
  3.7 1.0 %copy-start.2 = (f32[8,16,768]{2,1,0:T(8,128)S(1)}, f32[8,16,768]{2,1,0:T(8,128)}, u32[]{:S(2)}) copy-start(f32[8,16,768]{2,1,0:T(8,128)} %cgate_hbm.1) | copy-start | bytes 1179652
  4.7 0.9 %copy-start.3 = (bf16[1024,128]{1,0:T(8,128)(2,1)S(1)}, bf16[1024,128]{1,0:T(8,128)(2,1)}, u32[]{:S(2)}) copy-start(bf16[1024,128]{1,0:T(8,128)(2,1)} %key_hbm.1) | copy-start | bytes 786436
  5.6 0.9 %copy-start.4 = (bf16[1024,128]{1,0:T(8,128)(2,1)S(1)}, bf16[1024,128]{1,0:T(8,128)(2,1)}, u32[]{:S(2)}) copy-start(bf16[1024,128]{1,0:T(8,128)(2,1)} %value_hbm.1) | copy-start | bytes 786436
  6.6 0.7 %copy-start.5 = (bf16[8,1024]{1,0:T(8,128)(2,1)S(1)}, bf16[8,1024]{1,0:T(8,128)(2,1)}, u32[]{:S(2)}) copy-start(bf16[8,1024]{1,0:T(8,128)(2,1)} %tokens_hbm.1) | copy-start | bytes 49156
  7.3 0.7 %copy-start.6 = (f32[4096]{0:T(1024)S(1)}, f32[4096]{0:T(1024)}, u32[]{:S(2)}) copy-start(f32[4096]{0:T(1024)} %param.14) | copy-start | bytes 49156
  8.0 0.7 %copy-start.7 = (f32[8,16]{1,0:T(8,128)S(1)}, f32[8,16]{1,0:T(8,128)}, u32[]{:S(2)}) copy-start(f32[8,16]{1,0:T(8,128)} %total_hbm.1) | copy-start | bytes 1540
  8.7 0.7 %copy-start.8 = (f32[64]{0:T(128)S(1)}, f32[64]{0:T(128)}, u32[]{:S(2)}) copy-start(f32[64]{0:T(128)} %param.19) | copy-start | bytes 772
  9.4 0.7 %copy-start.9 = (s32[8]{0:T(128)S(1)}, s32[8]{0:T(128)}, u32[]{:S(2)}) copy-start(s32[8]{0:T(128)} %lengths_hbm.1) | copy-start | bytes 100

commit v2 on v1

--- a/solution.py
+++ b/solution.py
@@ -12,8 +12,10 @@
 LANES = 128
 SUBLANES = 8
 UNROLL_PEERS = 8
-QUERY_PIECES = 4
+QUERY_PIECES = 2
 CACHE_PIECES = 4
+BLOCK_PIECES = 1
+OUT_PIECES = 1
 NT = (((1,), (1,)), ((), ()))
 
 
@@ -41,9 +43,7 @@
     cgate_hbm,
     total_hbm,
     lengths_hbm,
-    mixed_ref,
-    knew_ref,
-    vnew_ref,
+    packed_ref,
     tokens_v,
     gain_v,
     query_v,
@@ -69,17 +69,20 @@
     recv1,
     send2,
     recv2,
-    send3,
-    recv3,
     send4,
     recv4,
 ):
+    sems1, sems2, sems4 = (
+        (send1, recv1),
+        (send2, recv2),
+        (send4, recv4),
+    )
     seqs, width = tokens_v.shape
     _, heads, positions = cgate_v.shape
     group = heads // 2
     qcols = query_v.shape[1]
     kcols = key_v.shape[1]
-    all_heads = gate_v.shape[1]
+    all_heads = gate_v.shape[0]
     kv = lax.axis_index("kv")
     tp = lax.axis_index("tp")
 
@@ -100,6 +103,9 @@
     greet("kv", kv, n_kv)
     greet("tp", tp, n_tp)
 
+    def span(start, size):
+        return (slice(None), pl.ds(start, size))
+
     slot = [0]
 
     def load(src, dst):
@@ -110,15 +116,14 @@
 
     c_tokens = load(tokens_hbm, tokens_v)
     c_gain = load(gain_hbm, gain_v)
-    rows = pl.ds(pl.multiple_of(kv * width, width), width)
-    c_gate = load(gate_hbm.at[rows], gate_v)
-    step = width // QUERY_PIECES
+    c_gate = load(gate_hbm if gate_hbm.shape == gate_v.shape else gate_hbm.at[:, pl.ds(pl.multiple_of(kv * width, width), width)], gate_v)
+    c_key = load(key_hbm, key_v)
+    c_value = load(value_hbm, value_v)
+    step = qcols // QUERY_PIECES
     c_query = [
-        load(query_hbm.at[pl.ds(i * step, step)], query_v.at[pl.ds(i * step, step)])
+        load(query_hbm.at[span(i * step, step)], query_v.at[span(i * step, step)])
         for i in range(QUERY_PIECES)
     ]
-    c_key = load(key_hbm, key_v)
-    c_value = load(value_hbm, value_v)
     c_bias = load(bias_hbm, bias_v)
     c_total = load(total_hbm, total_v)
     c_lengths = load(lengths_hbm, lengths_s)
@@ -132,34 +137,35 @@
         load(values_hbm.at[pl.ds(i * per, per)], values_v.at[pl.ds(i * per, per)])
         for i in range(CACHE_PIECES)
     ]
-    c_out = load(out_hbm, out_v)
-
-    def exchange(axis, me, n, buf, send, recv):
+    out_pieces = sems4[0].shape[0]
+    depth = width // out_pieces
+    c_out = [
+        load(out_hbm.at[pl.ds(i * depth, depth)], out_v.at[pl.ds(i * depth, depth)])
+        for i in range(out_pieces)
+    ]
+
+    def remote(axis, me, n, buf, sems, piece, cut, k, slot):
+        send, recv = sems
+        return pltpu.make_async_remote_copy(
+            src_ref=buf.at[me, *cut] if cut else buf.at[me],
+            dst_ref=buf.at[slot, *cut] if cut else buf.at[slot],
+            send_sem=send.at[piece, k],
+            recv_sem=recv.at[piece, slot],
+            device_id={axis: lax.rem(me + 1 + k, n)},
+            device_id_type=pl.DeviceIdType.MESH,
+        )
+
+    def exchange(axis, me, n, buf, sems, piece=0, cut=()):
         def one(k, c):
-            pltpu.make_async_remote_copy(
-                src_ref=buf.at[me],
-                dst_ref=buf.at[me],
-                send_sem=send.at[k],
-                recv_sem=recv.at[me],
-                device_id={axis: lax.rem(me + 1 + k, n)},
-                device_id_type=pl.DeviceIdType.MESH,
-            ).start()
+            remote(axis, me, n, buf, sems, piece, cut, k, me).start()
             return c
 
         fold(n - 1, one, 0)
 
-    def arrive(axis, me, n, buf, send, recv):
+    def arrive(axis, me, n, buf, sems, piece=0, cut=()):
         def one(k, c):
-            peer = lax.rem(me + 1 + k, n)
-            copy = pltpu.make_async_remote_copy(
-                src_ref=buf.at[me],
-                dst_ref=buf.at[peer],
-                send_sem=send.at[k],
-                recv_sem=recv.at[peer],
-                device_id={axis: peer},
-                device_id_type=pl.DeviceIdType.MESH,
-            )
-            copy.wait()
+            slot = lax.rem(me + 1 + k, n)
+            remote(axis, me, n, buf, sems, piece, cut, k, slot).wait()
             return c
 
         fold(n - 1, one, 0)
@@ -192,30 +198,29 @@
         return out[:seqs] + out[seqs:]
 
     c_gate.wait()
-    gates = project(gate_v[...])
-    base = qcols + 2 * kcols
+    gates = lax.dot_general(both, gate_v[...], NT, preferred_element_type=jnp.float32)
+    gates = gates[:seqs] + gates[seqs:]
+    base = 2 * kcols
+    side = base + 2 * LANES
     pair = jnp.concatenate(
         [gates, jnp.broadcast_to(squares, (seqs, LANES - all_heads))], axis=1
     )
     pair_high = pair.astype(jnp.bfloat16)
     parts[kv, :, base : base + LANES] = pair_high
-    parts[kv, :, base + LANES : base + 2 * LANES] = (
-        pair - pair_high.astype(jnp.float32)
-    ).astype(jnp.bfloat16)
-    acc = None
+    parts[kv, :, base + LANES : side] = (pair - pair_high.astype(jnp.float32)).astype(
+        jnp.bfloat16
+    )
+    c_key.wait()
+    parts[kv, :, :kcols] = project(key_v[...]).astype(jnp.bfloat16)
+    c_value.wait()
+    parts[kv, :, kcols:base] = project(value_v[...]).astype(jnp.bfloat16)
     for i in range(QUERY_PIECES):
         c_query[i].wait()
-        cut = slice(i * step, (i + 1) * step)
-        term = jnp.dot(both[:, cut], query_v[cut, :], preferred_element_type=jnp.float32)
-        acc = term if acc is None else acc + term
-    parts[kv, :, :qcols] = (acc[:seqs] + acc[seqs:]).astype(jnp.bfloat16)
-    c_key.wait()
-    parts[kv, :, qcols : qcols + kcols] = project(key_v[...]).astype(jnp.bfloat16)
-    c_value.wait()
-    parts[kv, :, qcols + kcols : base] = project(value_v[...]).astype(jnp.bfloat16)
-
+        parts[kv, :, side + i * step : side + (i + 1) * step] = project(
+            query_v[:, i * step : (i + 1) * step]
+        ).astype(jnp.bfloat16)
     pl.semaphore_wait(barrier, n_kv - 1 + n_tp - 1)
-    exchange("kv", kv, n_kv, parts, send1, recv1)
+    exchange("kv", kv, n_kv, parts, sems1)
 
     c_total.wait()
     c_lengths.wait()
@@ -230,20 +235,20 @@
             index < lengths_s[s], total_t[:, s : s + 1] - cgate_v[s], NEG_FILL
         )
 
-    arrive("kv", kv, n_kv, parts, send1, recv1)
+    arrive("kv", kv, n_kv, parts, sems1)
     summed = fold(
         n_kv,
         lambda j, c: c + parts[j].astype(jnp.float32),
-        jnp.zeros((seqs, base + 2 * LANES), jnp.float32),
-    )
-    pair = summed[:, base : base + LANES] + summed[:, base + LANES :]
+        jnp.zeros((seqs, side + qcols), jnp.float32),
+    )
+    pair = summed[:, base : base + LANES] + summed[:, base + LANES : side]
     scale = lax.rsqrt(pair[:, all_heads : all_heads + 1] / (width * n_kv) + 1e-6)
-    query = (summed[:, :qcols] * scale).astype(jnp.bfloat16).astype(jnp.float32)
+    query = (summed[:, side:] * scale).astype(jnp.bfloat16).astype(jnp.float32)
     query = query * (HEAD_SIZE ** -0.5)
-    knew = (summed[:, qcols : qcols + kcols] * scale).astype(jnp.bfloat16)
-    vnew = (summed[:, qcols + kcols : base] * scale).astype(jnp.bfloat16)
-    knew_ref[...] = knew
-    vnew_ref[...] = vnew
+    knew = (summed[:, :kcols] * scale).astype(jnp.bfloat16)
+    vnew = (summed[:, kcols:base] * scale).astype(jnp.bfloat16)
+    packed_ref[:, :kcols] = knew
+    packed_ref[:, kcols : 2 * kcols] = vnew
     knew = knew.astype(jnp.float32)
     vnew = vnew.astype(jnp.float32)
 
@@ -261,19 +266,18 @@
     def select(column):
         return jnp.where(low, column[:group], column[group:])
 
+    for copy in c_keys + c_values:
+        copy.wait()
     stat = jnp.zeros((group, LANES), jnp.float32)
     held = None
+    share = seqs // BLOCK_PIECES
     for s in range(seqs):
-        if s % per == 0:
-            c_keys[s // per].wait()
         q = qrows[pl.ds(s, heads, stride=seqs), :].astype(jnp.bfloat16)
         score = lax.dot_general(q, keys_v[s], NT, preferred_element_type=jnp.float32)
         score = score + cgate_v[s]
         peak = jnp.max(score, axis=1, keepdims=True)
         weight = jnp.exp(score - peak)
         mass = jnp.sum(weight, axis=1, keepdims=True)
-        if s % per == 0:
-            c_values[s // per].wait()
         value = jnp.dot(
             weight.astype(jnp.bfloat16), values_v[s], preferred_element_type=jnp.float32
         )
@@ -286,9 +290,18 @@
             blocks[kv, (s - 1) * group : (s + 1) * group, :] = jnp.concatenate(
                 [held, mine], axis=0
             ).astype(jnp.bfloat16)
-    stats[kv] = stat
-    exchange("kv", kv, n_kv, stats, send3, recv3)
-    exchange("kv", kv, n_kv, blocks, send2, recv2)
+        if s == seqs - 1:
+            left = stat
+            for i in range(2):
+                digits = []
+                for _ in range(2):
+                    digit = left.astype(jnp.bfloat16)
+                    left = left - digit.astype(jnp.float32)
+                    digits.append(digit)
+                first = seqs * group + 2 * i * group
+                blocks[kv, first : first + 2 * group, :] = jnp.concatenate(digits, axis=0)
+        if (s + 1) % share == 0:
+            exchange("kv", kv, n_kv, blocks, sems2)
 
     z = pair * scale
     z = z[:, :all_heads] + bias_v[...]
@@ -307,7 +320,17 @@
             own,
         )
 
-    arrive("kv", kv, n_kv, stats, send3, recv3)
+    arrive("kv", kv, n_kv, blocks, sems2)
+
+    def gather(j, c):
+        digits = blocks[j, seqs * group :, :].astype(jnp.float32)
+        total = digits[:group]
+        for i in range(1, 4):
+            total = total + digits[i * group : (i + 1) * group]
+        stats[j] = total
+        return c
+
+    fold(n_kv, gather, 0)
     peak = fold(
         n_kv - 1, lambda j, c: jnp.maximum(c, stats[j + 1]), stats[0]
     )
@@ -328,11 +351,10 @@
 
     own_weight = own_weight * inverse
     sums = [spread(own_weight, s) * vnew[s : s + 1, :] for s in range(seqs)]
-    arrive("kv", kv, n_kv, blocks, send2, recv2)
 
     def add(j, sums):
         a = factor(j) * inverse
-        block = blocks[j].astype(jnp.float32)
+        block = blocks[j, : seqs * group, :].astype(jnp.float32)
         return [
             sums[s] + spread(a, s) * block[s * group : (s + 1) * group]
             for s in range(seqs)
@@ -352,18 +374,30 @@
             pieces.append(jnp.where(low, pltpu.roll(first, HEAD_SIZE, 1), second))
     attended = jnp.concatenate(pieces, axis=1).astype(jnp.bfloat16)
 
-    c_out.wait()
-    mixes[tp] = lax.dot_general(
-        attended, out_v[...], NT, preferred_element_type=jnp.float32
-    ).astype(jnp.bfloat16)
-    exchange("tp", tp, n_tp, mixes, send4, recv4)
-    arrive("tp", tp, n_tp, mixes, send4, recv4)
+    for i in range(out_pieces):
+        c_out[i].wait()
+        mixes[tp, :, i * depth : (i + 1) * depth] = lax.dot_general(
+            attended,
+            out_v[i * depth : (i + 1) * depth, :],
+            NT,
+            preferred_element_type=jnp.float32,
+        ).astype(jnp.bfloat16)
+        exchange("tp", tp, n_tp, mixes, sems4, i, span(i * depth, depth))
+    for i in range(out_pieces):
+        arrive("tp", tp, n_tp, mixes, sems4, i, span(i * depth, depth))
     total = fold(
         n_tp,
         lambda j, c: c + mixes[j].astype(jnp.float32),
         jnp.zeros((seqs, width), jnp.float32),
     )
-    mixed_ref[...] = total.astype(jnp.bfloat16)
+    packed_ref[:, 2 * kcols :] = total.astype(jnp.bfloat16)
+
+
+def unpack(packed_ref, mixed_ref, knew_ref, vnew_ref):
+    kcols = knew_ref.shape[1]
+    knew_ref[...] = packed_ref[:, :kcols]
+    vnew_ref[...] = packed_ref[:, kcols : 2 * kcols]
+    mixed_ref[...] = packed_ref[:, 2 * kcols :]
 
 
 def per_device(n_kv, n_tp, *args):
@@ -386,10 +420,12 @@
     _, heads, positions = cache_gate.shape
     qcols, kcols = w_query.shape[1], key_weight.shape[1]
     all_heads = w_gate.shape[1]
+    gate = w_gate.T
     if width % LANES == 0:
         gain = norm_gain.reshape(-1, LANES)
     else:
         start = lax.axis_index("kv") * width
+        gate = lax.dynamic_slice_in_dim(gate, start, width, 1)
         gain = lax.dynamic_slice_in_dim(norm_gain, start, width, 0).reshape(1, width)
     bias = gate_bias.reshape(1, all_heads)
     operands = (
@@ -398,7 +434,7 @@
         w_query,
         key_weight,
         value_weight,
-        w_gate,
+        gate,
         bias,
         w_out,
         cache_keys,
@@ -410,24 +446,21 @@
     bf16, f32 = jnp.bfloat16, jnp.float32
     packed = qcols + 2 * kcols + 2 * LANES
     group = heads // 2
-    n_loads = 10 + QUERY_PIECES + 2 * CACHE_PIECES
+    out_pieces = OUT_PIECES if width % (OUT_PIECES * LANES) == 0 else 1
+    n_loads = 9 + QUERY_PIECES + 2 * CACHE_PIECES + out_pieces
     dma = pltpu.SemaphoreType.DMA
-    return pl.pallas_call(
+    results = pl.pallas_call(
         functools.partial(kernel, n_kv, n_tp),
-        out_shape=(
-            jax.ShapeDtypeStruct((seqs, width), bf16),
-            jax.ShapeDtypeStruct((seqs, kcols), bf16),
-            jax.ShapeDtypeStruct((seqs, kcols), bf16),
-        ),
-        in_specs=[pl.BlockSpec(memory_space=pl.ANY)] * len(operands),
-        out_specs=(pl.BlockSpec(memory_space=pltpu.VMEM),) * 3,
+        out_shape=pltpu.VMEM((seqs, width + 2 * kcols), bf16),
+        in_specs=[pl.BlockSpec(memory_space=pltpu.HBM)] * len(operands),
+        out_specs=pl.BlockSpec(memory_space=pltpu.VMEM),
         scratch_shapes=[
             pltpu.VMEM(tokens.shape, bf16),
             pltpu.VMEM(gain.shape, f32),
             pltpu.VMEM(w_query.shape, bf16),
             pltpu.VMEM(key_weight.shape, bf16),
             pltpu.VMEM(value_weight.shape, bf16),
-            pltpu.VMEM((width, all_heads), bf16),
+            pltpu.VMEM((all_heads, width), bf16),
             pltpu.VMEM(bias.shape, f32),
             pltpu.VMEM(w_out.shape, bf16),
             pltpu.VMEM(cache_keys.shape, bf16),
@@ -436,26 +469,36 @@
             pltpu.VMEM(gate_total.shape, f32),
             pltpu.SMEM(lengths.shape, jnp.int32),
             pltpu.VMEM((n_kv, seqs, packed), bf16),
-            pltpu.VMEM((n_kv, seqs * group, LANES), bf16),
+            pltpu.VMEM((n_kv, (seqs + 4) * group, LANES), bf16),
             pltpu.VMEM((n_kv, group, LANES), f32),
             pltpu.VMEM((n_tp, seqs, width), bf16),
             pltpu.VMEM((heads * seqs, LANES), f32),
             pltpu.VMEM((seqs * group, LANES), f32),
             pltpu.VMEM((LANES, LANES), f32),
             dma((n_loads,)),
-            dma((n_kv,)),
-            dma((n_kv,)),
-            dma((n_kv,)),
-            dma((n_kv,)),
-            dma((n_kv,)),
-            dma((n_kv,)),
-            dma((n_tp,)),
-            dma((n_tp,)),
+            dma((1, n_kv)),
+            dma((1, n_kv)),
+            dma((BLOCK_PIECES, n_kv)),
+            dma((BLOCK_PIECES, n_kv)),
+            dma((out_pieces, n_tp)),
+            dma((out_pieces, n_tp)),
         ],
         compiler_params=pltpu.CompilerParams(
-            collective_id=0, has_side_effects=True, vmem_limit_bytes=48 * 1024 * 1024
+            collective_id=0, has_side_effects=True, vmem_limit_bytes=67043328 - 64 * 1024
         ),
     )(*operands)
+    vmem = pl.BlockSpec(memory_space=pltpu.VMEM)
+    return pl.pallas_call(
+        unpack,
+        out_shape=(
+            jax.ShapeDtypeStruct((seqs, width), bf16),
+            jax.ShapeDtypeStruct((seqs, kcols), bf16),
+            jax.ShapeDtypeStruct((seqs, kcols), bf16),
+        ),
+        in_specs=[vmem],
+        out_specs=(vmem,) * 3,
+        compiler_params=pltpu.CompilerParams(vmem_limit_bytes=2 * 1024 * 1024),
+    )(results)
 
 
 def solution(mesh):

time: 33.3 us -> 21.8 us (0.65)
  local copies, waits for them, and re-layouts: 11.1 us -> 0 us
    unnamed x24 -> x0, local copies, waits for them, and re-layouts: 11.1 us -> none
    pallas_call x1 -> x2, Pallas kernels: 21.1 us -> 21 us  [the longest x1 20.3 us: per_device(): pl.pallas_call(functools.partial(kernel, n_kv, n_tp), out_shape=pltpu.VME...]
where the time goes in v2:
time: 21.8 us; the launch traced here: 21.6 us
  Pallas kernels  21 us (96%)
  between operations  0.64 us (3%)
    pallas_call x1, Pallas kernels, per_device(): pl.pallas_call(functools.partial(kernel, n_kv, n_tp), out_shape=pltpu.VME...  20.3 us
    pallas_call x1, Pallas kernels, per_device(): pl.pallas_call(unpack, out_shape=(jax.ShapeDtypeStruct((seqs, width), bf1...  0.61 us

profile of v2, /device:TPU:0, one launch (start us, length us, event | category | flops | bytes accessed | tf_op | source)
XLA Modules:
  0.0 21.6 jit_solution(3700312611553029161)
XLA Ops:
  0.6 20.3 %shard_map.148.packed_ref = bf16[8,1280]{1,0:T(8,128)(2,1)S(1)} custom-call(bf16[8,1024]{1,0:T(8,128)(2,1)} %tokens_hbm.1, f32[32,128]{1,0:T(8,128)} %bitcast.4, bf16[1024,1024]{1,0:T(8,128)(2,1)} %query_hbm.1, bf16[1024,128]{1,0:T(8,128)(2,1)} %key_hbm.1, bf16[1024,128]{1,0:T(8,128)(2,1)} %value_hbm.1, bf16[64,4096]{1,0:T(8,128)(2,1)} %bitcast.3, ...), custom_call_target="tpu_custom_call" | custom-call | tf_op jit(solution)/shard_map/pallas_call | solution.py:452
  21.0 0.6 %shard_map.149 = (bf16[8,1024]{1,0:T(8,128)(2,1)}, bf16[8,128]{1,0:T(8,128)(2,1)}, bf16[8,128]{1,0:T(8,128)(2,1)}) custom-call(bf16[8,1280]{1,0:T(8,128)(2,1)S(1)} %shard_map.148.packed_ref), custom_call_target="tpu_custom_call" | custom-call | tf_op jit(solution)/shard_map/pallas_call | solution.py:491
